TPU v7x, 512 devices: a whole 4x4x16 slice. The times are simulated.
512 devices in a mesh: sp: 32 (over z, core), tp: 16 (over y, x).
Axes of the slice: x: 4, y: 4, z: 16, core: 2. Of those that a mesh axis runs over, the one named last changes fastest.
Arguments:
- residual_in: bfloat16 [8192, 2048], P('sp'), may hold values from -3 to 3
- mix_gain: float32 [2048], replicated, may hold values from 0.1 to 1.9
- pool_weight: bfloat16 [512, 2048], P(None, 'tp'), may hold values from -0.5 to 0.5
- pool_scale: float32 [2048], P('tp'), may hold values from 0.1 to 1.9
- ffn_gain: float32 [2048], replicated, may hold values from 0.1 to 1.9
- route_ids: int32 [8192, 2], P('sp'), may hold values from 0 to 31, all different within a row; in each aligned block of 16 rows (0 to 15, 16 to 31, ...) at most 2 rows name the same one
- route_weights: float32 [8192, 2], P('sp'), may hold values from 0.1 to 1
- gate_weight: bfloat16 [32, 2048, 3584], P('sp', None, 'tp'), may hold values from -0.125 to 0.125
- up_weight: bfloat16 [32, 2048, 3584], P('sp', None, 'tp'), may hold values from -0.125 to 0.125
- down_weight: bfloat16 [32, 3584, 2048], P('sp', 'tp'), may hold values from -0.09375 to 0.09375
Outputs:
- layer_out: bfloat16 [8192, 2048], P('sp')
Inputs may be any that keep to these rules, and one draw needn't show every extreme that they name: `route_ids`: each row names 2 different experts; in each aligned block of 16 rows no expert is named by more than 2 rows, and some block has an expert named by exactly 2 rows.
All inputs are finite; a program needn't handle non-finite values.
Results may differ from a plain program's by a relative error of at most 0.0074.
Values may be sent and summed in bfloat16 or wider, within the bound.
No kernel may reach another device: no remote copies, remote signals or barrier semaphores. Data moves between devices by JAX's collectives and lax.ppermute only.
A program may use at most 64 MiB of HBM per device.

v0:
```python
import jax
import jax.numpy as jnp
from jax import lax
from jax.sharding import Mesh
from jax.sharding import PartitionSpec as P

GROUPS = 4
SPAN = 16
TOP_K = 2
SP = ("sp_0", "sp_1")
EPS = 1e-06


def from_behind(value, axis, steps):
    count = lax.axis_size(axis)
    first, last = (max(0, -steps), min(count, count - steps))
    return lax.ppermute(value, axis, [(source, source + steps) for source in range(first, last)])


def split_up(shard, dim, size):
    before, after = (shard.shape[:dim], shard.shape[dim + 1 :])
    return jnp.moveaxis(shard.reshape(*before, size, -1, *after), dim, 0)


def sent_and_summed(shard, axis, dim):
    size = lax.axis_size(axis)
    blocks = lax.all_to_all(split_up(shard, dim, size), axis, 0, 0, tiled=True)
    return jnp.sum(blocks.astype(jnp.float32), axis=0)


def in_order(blocks, dim):
    dims = list(blocks.shape[1:])
    dims[dim] *= blocks.shape[0]
    return jnp.moveaxis(blocks, 0, dim).reshape(dims)


def exchange_in_order(blocks, axes, order):
    dims = [lax.axis_size(a) for a in axes]
    blocks = blocks.reshape(*dims, *blocks.shape[1:])
    for k in order:
        blocks = lax.all_to_all(blocks, axes[k], split_axis=k, concat_axis=k, tiled=True)
    return blocks.reshape(-1, *blocks.shape[len(axes) :])


def core_and_chips(shard, groups, order, split_dim, concat_dim):
    size = lax.axis_size(groups[0]) * lax.axis_size(groups[1])
    blocks = split_up(shard, split_dim, size)
    return in_order(exchange_in_order(blocks, groups, order), concat_dim)


def copy_for_each(shard, axis):
    size = lax.axis_size(axis)
    return lax.all_to_all(
        jnp.broadcast_to(shard[None], (size, *shard.shape)), axis, 0, 0, tiled=True
    )


def gather_directly(shard, axis, dim):
    blocks = copy_for_each(shard, axis)
    return in_order(blocks, dim)


def rms_scale(values, gain):
    return values * lax.rsqrt(jnp.mean(values * values, axis=-1, keepdims=True) + EPS) * gain


def slot_table(chosen_ids, experts, capacity):
    flat_ids = chosen_ids.reshape(-1)
    matches = (flat_ids[:, None] == jnp.arange(experts, dtype=jnp.int32)[None, :]).astype(jnp.int32)
    before = jnp.cumsum(matches, axis=0) - matches
    slot_of = jnp.sum(before * matches, axis=1)
    target = flat_ids * capacity + slot_of
    return (target[:, None] == jnp.arange(experts * capacity, dtype=jnp.int32)[None, :]).astype(
        jnp.float32
    )


def shards(
    residual_in,
    mix_gain,
    pool_weight,
    pool_scale,
    ffn_gain,
    route_ids,
    route_weights,
    gate_weight,
    up_weight,
    down_weight,
):
    tp_count = lax.axis_size("tp")
    sp_count = lax.axis_size(SP)
    tp_index = lax.axis_index("tp")
    tok_count, width = residual_in.shape
    group_width = width // GROUPS
    col_count = pool_weight.shape[1]
    row_count = tok_count // tp_count
    capacity = 2 * TOP_K * row_count // sp_count
    group_index = tp_index * col_count // group_width
    window = jnp.power(2, group_index + 1)
    stream = residual_in.astype(jnp.float32)
    inverse = lax.rsqrt(jnp.mean(stream * stream, axis=-1, keepdims=True) + EPS)
    stream_group = lax.dynamic_slice_in_dim(stream, group_index * group_width, group_width, 1)
    gain_group = lax.dynamic_slice_in_dim(mix_gain, group_index * group_width, group_width, 0)
    normed_group = (stream_group * inverse * gain_group).astype(jnp.bfloat16)
    rim_rows = from_behind(normed_group[tok_count - SPAN :], SP, 1)
    extended = jnp.concatenate([rim_rows, normed_group], axis=0).astype(jnp.float32)
    window_sum = jnp.zeros((tok_count, group_width), jnp.float32)
    for offset in range(SPAN):
        window_sum = window_sum + jnp.where(
            offset < window, extended[SPAN - offset : SPAN - offset + tok_count], 0.0
        )
    position = lax.axis_index(SP) * tok_count + jnp.arange(tok_count, dtype=jnp.int32)
    divisor = jnp.minimum(position + 1, window).astype(jnp.float32)
    pooled = (window_sum / divisor[:, None] - extended[SPAN:]).astype(jnp.bfloat16)
    mixed = (jnp.dot(pooled, pool_weight, preferred_element_type=jnp.float32) * pool_scale).astype(
        jnp.bfloat16
    )
    stream_own = lax.dynamic_slice_in_dim(stream, tp_index * row_count, row_count, 0)
    mixed_own = lax.all_to_all(mixed, "tp", split_axis=0, concat_axis=1, tiled=True)
    after_own = (stream_own + mixed_own.astype(jnp.float32)).astype(jnp.bfloat16)
    normed_own = rms_scale(after_own.astype(jnp.float32), ffn_gain).astype(jnp.bfloat16)
    ids_own = lax.dynamic_slice_in_dim(route_ids, tp_index * row_count, row_count, 0)
    table_own = slot_table(ids_own, sp_count, capacity)
    repeated = jnp.repeat(normed_own, TOP_K, axis=0)
    outgoing = lax.dot_general(
        table_own.astype(jnp.bfloat16),
        repeated,
        (((0,), (0,)), ((), ())),
        preferred_element_type=jnp.float32,
    )
    outgoing = outgoing.astype(jnp.bfloat16).reshape(sp_count, capacity, width)
    arrived = lax.all_to_all(outgoing, SP, split_axis=0, concat_axis=0, tiled=True)
    piece = lax.all_gather(arrived, "tp", axis=0, tiled=True)
    flat_rows = piece.reshape(-1, width)
    gate_part = jnp.dot(flat_rows, gate_weight[0], preferred_element_type=jnp.float32)
    up_part = jnp.dot(flat_rows, up_weight[0], preferred_element_type=jnp.float32)
    hidden = (jax.nn.silu(gate_part) * up_part).astype(jnp.bfloat16)
    hidden_all = hidden.reshape(piece.shape[0], piece.shape[1], hidden.shape[1])
    hidden_flat = hidden_all.reshape(-1, hidden_all.shape[-1])
    term = jnp.dot(hidden_flat, down_weight[0], preferred_element_type=jnp.float32)
    summed = sent_and_summed(
        term.astype(jnp.bfloat16).astype(jnp.float32).astype(jnp.bfloat16), "tp", 0
    )
    expert_out = summed.astype(jnp.bfloat16).reshape(sp_count, capacity, width)
    returned_rows = core_and_chips(expert_out, ("sp_0", "sp_1"), (1, 0), 0, 0)
    weights_own = lax.dynamic_slice_in_dim(route_weights, tp_index * row_count, row_count, 0)
    weight_table = jnp.einsum(
        "rk,rkc->rc", weights_own, table_own.reshape(row_count, TOP_K, sp_count * capacity)
    )
    expert_mix = jnp.dot(
        weight_table,
        returned_rows.reshape(-1, width).astype(jnp.float32),
        precision=lax.Precision.HIGHEST,
    )
    out_own = (after_own.astype(jnp.float32) + expert_mix).astype(jnp.bfloat16)
    return gather_directly(out_own, "tp", 0)


def solution(mesh):
    torus = Mesh(mesh.devices.reshape(16, 2, mesh.shape["tp"]), ("sp_0", "sp_1", "tp"))
    return jax.shard_map(
        shards,
        mesh=torus,
        in_specs=(
            P(SP, None),
            P(),
            P(None, "tp"),
            P("tp"),
            P(),
            P(SP, None),
            P(SP, None),
            P(SP, None, "tp"),
            P(SP, None, "tp"),
            P(SP, "tp", None),
        ),
        out_specs=P(SP, None),
        check_vma=False,
    )
```

profile of v0, /device:TPU:32, one launch (start us, length us, event | category | flops | bytes accessed | tf_op | source)
XLA Modules:
  0.0 268.7 jit_solution(1426922073096499499)
XLA Ops:
  6.5 1.6 multiply_reduce_fusion
  8.1 1.5 convert_element_type.67
  9.6 0.8 dynamic_slice.17
  10.4 0.1 multiply_convert_fusion
  10.5 1.9 collective-permute-start
  12.5 0.1 constant_dynamic-slice_fusion
  12.6 0.1 copy.24
  12.7 0.1 eq.35
  12.8 0.1 fusion.40
  12.8 0.1 reduce_window_sum.11
  12.9 0.2 select_reduce_fusion
  13.1 2.5 collective-permute-done
  15.6 0.1 maximum_convert_fusion
  15.7 0.0 copy-start.1
  15.7 2.0 fusion.2
  17.7 7.0 %all-to-all-start = ((bf16[16,16,128]{2,1,0:T(8,128)(2,1)}), bf16[16,16,128]{2,1,0:T(8,128)(2,1)S(1)}, u32[]{:S(2)}, u32[]{:S(2)}) async-start(bf16[16,16,128]{2,1,0:T(8,128)(2,1)} %bitcast), calls=%async_computation | async-start | bytes 131072 | tf_op jit(solution)/shard_map/all_to_all | solution.py:119
  24.8 0.0 all-gather.2.cloned.1.call-start
  24.8 7.6 %all-to-all-done = bf16[16,16,128]{2,1,0:T(8,128)(2,1)S(1)} async-done(((bf16[16,16,128]{2,1,0:T(8,128)(2,1)}), bf16[16,16,128]{2,1,0:T(8,128)(2,1)S(1)}, u32[]{:S(2)}, u32[]{:S(2)}) %all-to-all-start) | async-done | bytes 65568 | tf_op jit(solution)/shard_map/all_to_all | solution.py:119
  32.4 0.1 fusion.33
  32.6 0.1 fusion.35
  32.7 0.1 broadcast_in_dim.38
  32.8 0.1 reshape.67
  32.8 0.3 convolution_convert_fusion.1
  33.2 0.2 reshape.68
  33.3 37.4 %all_to_all.38 = bf16[32,2,2048]{2,1,0:T(2,128)(2,1)} all-to-all(bf16[32,2,2048]{2,1,0:T(2,128)(2,1)S(1)} %reshape.68), channel_id=1, replica_groups=mesh['sp_0'=16,'sp_1'=2,'tp'=16] {'sp_0','sp_1'}, dimensions={0} | all-to-all | bytes 524288 | tf_op jit(solution)/shard_map/all_to_all | solution.py:132
  70.8 0.0 all-gather.2.cloned.1.call-update
  70.8 0.0 copy-start.3
  70.8 56.0 %all-gather.2.cloned.1.call-done = bf16[512,2,2048]{2,1,0:T(2,128)(2,1)} async-done(((bf16[32,2,2048]{2,1,0:T(2,128)(2,1)}), bf16[512,2,2048]{2,1,0:T(2,128)(2,1)}) %all-gather.2.cloned.1.call-update) | async-done | bytes 4194320 | tf_op jit(solution)/shard_map/all_gather | solution.py:133
  126.8 7.2 %reshape.69 = bf16[1024,2048]{1,0:T(8,128)(2,1)} reshape(bf16[512,2,2048]{2,1,0:T(2,128)(2,1)} %all-gather.2.cloned.1.call-done) | data formatting | bytes 8388608 | tf_op jit(solution)/shard_map/reshape | solution.py:134
  134.0 4.6 %fusion.6 = f32[1024,224]{0,1:T(8,128)} fusion(bf16[1024,2048]{1,0:T(8,128)(2,1)} %reshape.69, bf16[1,2048,224]{1,2,0:T(8,128)(2,1)S(1)} %copy-done.3), kind=kOutput, calls=%fused_computation.11 | convolution fusion | flops 939524096 | bytes 6029312 | tf_op jit(solution)/shard_map/dot_general | solution.py:135
  138.6 7.0 %convolution_convert_fusion = bf16[1024,2048]{1,0:T(8,128)(2,1)} fusion(bf16[1024,2048]{1,0:T(8,128)(2,1)} %reshape.69, bf16[1,224,2048]{2,1,0:T(8,128)(2,1)S(1)} %copy-done, bf16[1,2048,224]{1,2,0:T(8,128)(2,1)S(1)} %copy-done.4, f32[1024,224]{0,1:T(8,128)} %fusion.6), kind=kOutput, calls=%fused_computation | convolution fusion | flops 1882521600 | bytes 11141120 | tf_op jit(solution)/shard_map/dot_general | solution.py:140
  145.6 56.0 %all_to_all.39 = bf16[16,64,2048]{2,1,0:T(8,128)(2,1)} all-to-all(bf16[16,64,2048]{2,1,0:T(8,128)(2,1)} %bitcast.35), channel_id=1, replica_groups=mesh['sp_0'=16,'sp_1'=2,'tp'=16] {'tp'}, dimensions={0} | all-to-all | bytes 8388608 | tf_op jit(solution)/shard_map/all_to_all | solution.py:27
  201.7 3.0 %reduce_sum.45 = bf16[64,2048]{1,0:T(8,128)(2,1)S(1)} reduce(bf16[16,64,2048]{2,1,0:T(8,128)(2,1)} %all_to_all.39, bf16[]{:T(256)} %constant.97.clone.1), dimensions={0}, to_apply=%region_4.5 | reduce | flops 1966080 | bytes 4456450 | tf_op jit(solution)/shard_map/reduce_sum | solution.py:28
  204.6 0.2 reshape_reshape_reshape.6
  204.8 0.2 copy.20
  205.0 3.9 %all_to_all.40 = bf16[16,2,1,2,2048]{4,3,0,2,1:T(2,128)(2,1)S(1)} all-to-all(bf16[16,2,1,2,2048]{4,3,0,2,1:T(2,128)(2,1)S(1)} %copy.20), channel_id=1, replica_groups=mesh['sp_0'=16,'sp_1'=2,'tp'=16] {'sp_1'}, dimensions={1} | all-to-all | bytes 524288 | tf_op jit(solution)/shard_map/all_to_all | solution.py:41
  209.0 1.0 copy.21
  209.9 12.7 %all-to-all-start.4 = ((bf16[16,2,1,2,2048]{4,3,1,2,0:T(2,128)(2,1)}), bf16[16,2,1,2,2048]{4,3,1,2,0:T(2,128)(2,1)S(1)}, u32[]{:S(2)}, u32[]{:S(2)}) async-start(bf16[16,2,1,2,2048]{4,3,1,2,0:T(2,128)(2,1)} %copy.21), calls=%async_computation.4 | async-start | bytes 524288 | tf_op jit(solution)/shard_map/all_to_all | solution.py:41
  222.6 0.1 reduce_sum.43
  222.7 0.8 dynamic-slice_bitcast_fusion
  223.4 0.1 copy.22
  223.5 0.2 fusion.37
  223.7 17.2 %all-to-all-done.4 = bf16[16,2,1,2,2048]{4,3,1,2,0:T(2,128)(2,1)S(1)} async-done(((bf16[16,2,1,2,2048]{4,3,1,2,0:T(2,128)(2,1)}), bf16[16,2,1,2,2048]{4,3,1,2,0:T(2,128)(2,1)S(1)}, u32[]{:S(2)}, u32[]{:S(2)}) %all-to-all-start.4) | async-done | bytes 262176 | tf_op jit(solution)/shard_map/all_to_all | solution.py:41
  241.0 0.1 reshape_reshape_reshape.7
  241.1 0.2 fusion
  241.3 0.1 broadcast_in_dim.39
  241.4 19.5 %all_to_all.41 = bf16[16,16,2048]{2,1,0:T(8,128)(2,1)S(1)} all-to-all(bf16[16,16,2048]{2,1,0:T(8,128)(2,1)S(1)} %broadcast_in_dim.39), channel_id=1, replica_groups=mesh['sp_0'=16,'sp_1'=2,'tp'=16] {'tp'}, dimensions={0} | all-to-all | bytes 2097152 | tf_op jit(solution)/shard_map/all_to_all | solution.py:53
  260.9 1.0 copy.29
  (18 shorter events, 0.1 us)
Async XLA Ops:
  6.5 132.1 %copy-start = (bf16[1,224,2048]{2,1,0:T(8,128)(2,1)S(1)}, bf16[1,224,2048]{2,1,0:T(8,128)(2,1)}, u32[]{:S(2)}) copy-start(bf16[1,224,2048]{2,1,0:T(8,128)(2,1)} %param.19) | copy-start | bytes 2752516
  6.5 6.0 %copy-start.2 = (s32[256,2]{0,1:T(2,128)S(1)}, s32[256,2]{0,1:T(2,128)}, u32[]{:S(2)}) copy-start(s32[256,2]{0,1:T(2,128)} %param.15) | copy-start | bytes 6148
  6.5 9.1 %copy-start.6 = (f32[128]{0:T(128)S(1)}, f32[128]{0:T(128)}, u32[]{:S(2)}) copy-start(f32[128]{0:T(128)} %param.13) | copy-start | bytes 1540
  6.5 9.1 %copy-start.5 = (bf16[512,128]{1,0:T(8,128)(2,1)S(1)}, bf16[512,128]{1,0:T(8,128)(2,1)}, u32[]{:S(2)}) copy-start(bf16[512,128]{1,0:T(8,128)(2,1)} %param.12) | copy-start | bytes 393220
  10.5 5.1 %collective-permute-start = (bf16[16,512]{1,0:T(8,128)(2,1)S(1)}, bf16[16,512]{1,0:T(8,128)(2,1)S(1)}, u32[]{:S(2)}, u32[]{:S(2)}) collective-permute-start(bf16[16,512]{1,0:T(8,128)(2,1)S(1)} %slice.69), channel_id=1, source_target_pairs={{0,16},{16,32},{32,48},{48,64},{64,80},{80,96},{96,112},{112,128},... | collective-permute-start | bytes 49160 | tf_op jit(solution)/shard_map/ppermute | solution.py:17
  15.7 16.9 %copy-start.1 = (f32[2048]{0:T(1024)S(1)}, f32[2048]{0:T(1024)}, u32[]{:S(2)}) copy-start(f32[2048]{0:T(1024)} %param.14) | copy-start | bytes 24580
  17.7 14.7 %all-to-all-start = ((bf16[16,16,128]{2,1,0:T(8,128)(2,1)}), bf16[16,16,128]{2,1,0:T(8,128)(2,1)S(1)}, u32[]{:S(2)}, u32[]{:S(2)}) async-start(bf16[16,16,128]{2,1,0:T(8,128)(2,1)} %bitcast), calls=%async_computation | async-start | bytes 131072 | tf_op jit(solution)/shard_map/all_to_all | solution.py:119
  24.8 102.0 %all-gather.2.cloned.1.call-start = ((), (), s32[]{:S(2)}) async-start(), calls=%async_computation.6 | async-start | bytes 4456448 | tf_op jit(solution)/shard_map/all_gather | solution.py:133
  70.8 63.2 %copy-start.3 = (bf16[1,2048,224]{1,2,0:T(8,128)(2,1)S(1)}, bf16[1,2048,224]{1,2,0:T(8,128)(2,1)}, u32[]{:S(2)}) copy-start(bf16[1,2048,224]{1,2,0:T(8,128)(2,1)} %param.17) | copy-start | bytes 2752516
  134.0 4.6 %copy-start.4 = (bf16[1,2048,224]{1,2,0:T(8,128)(2,1)S(1)}, bf16[1,2048,224]{1,2,0:T(8,128)(2,1)}, u32[]{:S(2)}) copy-start(bf16[1,2048,224]{1,2,0:T(8,128)(2,1)} %param.18) | copy-start | bytes 2752516
  209.9 31.0 %all-to-all-start.4 = ((bf16[16,2,1,2,2048]{4,3,1,2,0:T(2,128)(2,1)}), bf16[16,2,1,2,2048]{4,3,1,2,0:T(2,128)(2,1)S(1)}, u32[]{:S(2)}, u32[]{:S(2)}) async-start(bf16[16,2,1,2,2048]{4,3,1,2,0:T(2,128)(2,1)} %copy.21), calls=%async_computation.4 | async-start | bytes 524288 | tf_op jit(solution)/shard_map/all_to_all | solution.py:41
Sparse Core Ops, SparseCore 0:
  70.9 55.8 all-gather.1
where the time goes:
time: 269 us
  blocking collectives  117 us (43%)
  waiting for transfers between devices  83.3 us (31%)
  starting transfers between devices  21.7 us (8%)
  matrix products  14.4 us (5%)
  between operations  13.7 us (5%)
  local copies, waits for them, and re-layouts  12 us (4%)
  other arithmetic  6.75 us (3%)
    all_to_all x1, blocking collectives, sent_and_summed(): blocks = lax.all_to_all(split_up(shard, dim, size), axis, 0, 0, tiled=True)  56 us
    all_gather x1, waiting for transfers between devices, shards(): piece = lax.all_gather(arrived, 'tp', axis=0, tiled=True)  56 us
    all_to_all x1, blocking collectives, shards(): lax.all_to_all(outgoing, SP, split_axis=0, concat_axis=0, tiled=True)  37.4 us
    all_to_all x1, blocking collectives, copy_for_each(): lax.all_to_all(jnp.broadcast_to(shard[None], (size, *shard.shape)), axis,...  19.5 us
    all_to_all x1, waiting for transfers between devices, exchange_in_order(): lax.all_to_all(blocks, axes[k], split_axis=k, concat_axis=k, tiled=True)  17.2 us
    all_to_all x1, starting transfers between devices, exchange_in_order(): lax.all_to_all(blocks, axes[k], split_axis=k, concat_axis=k, tiled=True)  12.7 us
    all_to_all x1, waiting for transfers between devices, shards(): lax.all_to_all(mixed, 'tp', split_axis=0, concat_axis=1, tiled=True)  7.6 us
    reshape x1, local copies, waits for them, and re-layouts, shards(): flat_rows = piece.reshape(-1, width)  7.21 us
  transfers between devices with their start and end apart: 4, of which 4 were waited for; matrix products, arithmetic and copies ran while one was open for 1% of the time, Pallas kernels for 0%

commit v1 on v0

--- a/solution.py
+++ b/solution.py
@@ -116,7 +116,9 @@
         jnp.bfloat16
     )
     stream_own = lax.dynamic_slice_in_dim(stream, tp_index * row_count, row_count, 0)
-    mixed_own = lax.all_to_all(mixed, "tp", split_axis=0, concat_axis=1, tiled=True)
+    mixed_own = jnp.concatenate(
+        lax.all_to_all(jnp.stack(jnp.split(mixed, lax.axis_size("tp"), axis=0)), "tp", 0, 0), axis=1
+    )
     after_own = (stream_own + mixed_own.astype(jnp.float32)).astype(jnp.bfloat16)
     normed_own = rms_scale(after_own.astype(jnp.float32), ffn_gain).astype(jnp.bfloat16)
     ids_own = lax.dynamic_slice_in_dim(route_ids, tp_index * row_count, row_count, 0)

time: 269 us -> 278 us (1.033)
  local copies, waits for them, and re-layouts: 12 us -> 21.5 us
    unnamed x16 -> x31, local copies, waits for them, and re-layouts: 1.09 us -> 9.99 us
where the time goes in v1:
time: 278 us
  blocking collectives  117 us (42%)
  waiting for transfers between devices  83.3 us (30%)
  starting transfers between devices  21.7 us (8%)
  local copies, waits for them, and re-layouts  21.5 us (8%)
  matrix products  13.7 us (5%)
  between operations  13.7 us (5%)
  other arithmetic  6.75 us (2%)
    all_to_all x1, blocking collectives, sent_and_summed(): blocks = lax.all_to_all(split_up(shard, dim, size), axis, 0, 0, tiled=True)  56.1 us
    all_gather x1, waiting for transfers between devices, shards(): piece = lax.all_gather(arrived, 'tp', axis=0, tiled=True)  56 us
    all_to_all x1, blocking collectives, shards(): lax.all_to_all(outgoing, SP, split_axis=0, concat_axis=0, tiled=True)  37.4 us
    all_to_all x1, blocking collectives, copy_for_each(): lax.all_to_all(jnp.broadcast_to(shard[None], (size, *shard.shape)), axis,...  19.5 us
    all_to_all x1, waiting for transfers between devices, exchange_in_order(): lax.all_to_all(blocks, axes[k], split_axis=k, concat_axis=k, tiled=True)  17.2 us
    all_to_all x1, starting transfers between devices, exchange_in_order(): lax.all_to_all(blocks, axes[k], split_axis=k, concat_axis=k, tiled=True)  12.7 us
    unnamed x31, local copies, waits for them, and re-layouts  9.99 us
    all_to_all x1, waiting for transfers between devices, shards(): lax.all_to_all(jnp.stack(jnp.split(mixed, lax.axis_size('tp'), axis=0)),...  7.61 us
  transfers between devices with their start and end apart: 4, of which 4 were waited for; matrix products, arithmetic and copies ran while one was open for 1% of the time, Pallas kernels for 0%

profile of v1, /device:TPU:32, one launch (start us, length us, event | category | flops | bytes accessed | tf_op | source)
XLA Modules:
  0.0 277.6 jit_solution(8813035531677727605)
XLA Ops:
  6.5 1.6 multiply_reduce_fusion
  8.1 1.5 convert_element_type.67
  9.6 0.8 dynamic_slice.17
  10.4 0.1 multiply_convert_fusion
  10.5 1.9 collective-permute-start
  12.9 0.2 select_reduce_fusion
  13.1 2.5 collective-permute-done
  15.7 1.4 fusion.2
  17.1 0.6 constant_dynamic-update-slice_fusion.15
  17.7 0.6 constant_dynamic-update-slice_fusion.14
  18.3 0.6 constant_dynamic-update-slice_fusion.13
  18.9 0.6 constant_dynamic-update-slice_fusion.12
  19.5 0.6 constant_dynamic-update-slice_fusion.11
  20.1 0.6 constant_dynamic-update-slice_fusion.10
  20.7 0.6 constant_dynamic-update-slice_fusion.9
  21.3 0.6 constant_dynamic-update-slice_fusion.8
  21.8 0.6 constant_dynamic-update-slice_fusion.7
  22.4 0.6 constant_dynamic-update-slice_fusion.6
  23.0 0.6 constant_dynamic-update-slice_fusion.5
  23.6 0.6 constant_dynamic-update-slice_fusion.4
  24.2 0.6 constant_dynamic-update-slice_fusion.3
  24.8 0.6 constant_dynamic-update-slice_fusion.2
  25.4 0.6 constant_dynamic-update-slice_fusion.1
  26.0 0.6 constant_dynamic-update-slice_fusion
  26.6 7.0 %all-to-all-start = ((bf16[16,16,128]{2,1,0:T(8,128)(2,1)}), bf16[16,16,128]{2,1,0:T(8,128)(2,1)S(1)}, u32[]{:S(2)}, u32[]{:S(2)}) async-start(bf16[16,16,128]{2,1,0:T(8,128)(2,1)} %constant_dynamic-update-slice_fusion), calls=%async_computation | async-start | bytes 131072 | tf_op jit(solution)/shard_map/all_to_all | solution.py:120
  33.7 7.6 %all-to-all-done = bf16[16,16,128]{2,1,0:T(8,128)(2,1)S(1)} async-done(((bf16[16,16,128]{2,1,0:T(8,128)(2,1)}), bf16[16,16,128]{2,1,0:T(8,128)(2,1)S(1)}, u32[]{:S(2)}, u32[]{:S(2)}) %all-to-all-start) | async-done | bytes 65568 | tf_op jit(solution)/shard_map/all_to_all | solution.py:120
  41.3 0.1 fusion.33
  41.7 0.3 convolution_convert_fusion.1
  42.0 0.2 reshape.67
  42.2 37.4 %all_to_all.30 = bf16[32,2,2048]{2,1,0:T(2,128)(2,1)} all-to-all(bf16[32,2,2048]{2,1,0:T(2,128)(2,1)S(1)} %reshape.67), channel_id=1, replica_groups=mesh['sp_0'=16,'sp_1'=2,'tp'=16] {'sp_0','sp_1'}, dimensions={0} | all-to-all | bytes 524288 | tf_op jit(solution)/shard_map/all_to_all | solution.py:134
  79.7 56.0 %all-gather.2.cloned.1.call-done = bf16[512,2,2048]{2,1,0:T(2,128)(2,1)} async-done(((bf16[32,2,2048]{2,1,0:T(2,128)(2,1)}), bf16[512,2,2048]{2,1,0:T(2,128)(2,1)}) %all-gather.2.cloned.1.call-update) | async-done | bytes 4194320 | tf_op jit(solution)/shard_map/all_gather | solution.py:135
  135.7 7.2 %reshape.68 = bf16[1024,2048]{1,0:T(8,128)(2,1)} reshape(bf16[512,2,2048]{2,1,0:T(2,128)(2,1)} %all-gather.2.cloned.1.call-done) | data formatting | bytes 8388608 | tf_op jit(solution)/shard_map/reshape | solution.py:136
  142.9 4.6 %fusion.6 = f32[1024,224]{0,1:T(8,128)} fusion(bf16[1024,2048]{1,0:T(8,128)(2,1)} %reshape.68, bf16[1,2048,224]{1,2,0:T(8,128)(2,1)S(1)} %copy-done.3), kind=kOutput, calls=%fused_computation.11 | convolution fusion | flops 939524096 | bytes 6029312 | tf_op jit(solution)/shard_map/dot_general | solution.py:137
  147.5 7.0 %convolution_convert_fusion = bf16[1024,2048]{1,0:T(8,128)(2,1)} fusion(bf16[1024,2048]{1,0:T(8,128)(2,1)} %reshape.68, bf16[1,224,2048]{2,1,0:T(8,128)(2,1)S(1)} %copy-done, bf16[1,2048,224]{1,2,0:T(8,128)(2,1)S(1)} %copy-done.4, f32[1024,224]{0,1:T(8,128)} %fusion.6), kind=kOutput, calls=%fused_computation | convolution fusion | flops 1882521600 | bytes 11141120 | tf_op jit(solution)/shard_map/dot_general | solution.py:142
  154.4 56.1 %all_to_all.31 = bf16[16,64,2048]{2,1,0:T(8,128)(2,1)} all-to-all(bf16[16,64,2048]{2,1,0:T(8,128)(2,1)} %bitcast.98), channel_id=1, replica_groups=mesh['sp_0'=16,'sp_1'=2,'tp'=16] {'tp'}, dimensions={0} | all-to-all | bytes 8388608 | tf_op jit(solution)/shard_map/all_to_all | solution.py:27
  210.5 3.0 %reduce_sum.45 = bf16[64,2048]{1,0:T(8,128)(2,1)S(1)} reduce(bf16[16,64,2048]{2,1,0:T(8,128)(2,1)} %all_to_all.31, bf16[]{:T(256)} %constant.97.clone.1), dimensions={0}, to_apply=%region_4.5 | reduce | flops 1966080 | bytes 4456450 | tf_op jit(solution)/shard_map/reduce_sum | solution.py:28
  213.5 0.2 reshape_reshape_reshape.6
  213.7 0.2 copy.19
  213.9 3.9 %all_to_all.32 = bf16[16,2,1,2,2048]{4,3,0,2,1:T(2,128)(2,1)S(1)} all-to-all(bf16[16,2,1,2,2048]{4,3,0,2,1:T(2,128)(2,1)S(1)} %copy.19), channel_id=1, replica_groups=mesh['sp_0'=16,'sp_1'=2,'tp'=16] {'sp_1'}, dimensions={1} | all-to-all | bytes 524288 | tf_op jit(solution)/shard_map/all_to_all | solution.py:41
  217.8 1.0 copy.20
  218.8 12.7 %all-to-all-start.4 = ((bf16[16,2,1,2,2048]{4,3,1,2,0:T(2,128)(2,1)}), bf16[16,2,1,2,2048]{4,3,1,2,0:T(2,128)(2,1)S(1)}, u32[]{:S(2)}, u32[]{:S(2)}) async-start(bf16[16,2,1,2,2048]{4,3,1,2,0:T(2,128)(2,1)} %copy.20), calls=%async_computation.4 | async-start | bytes 524288 | tf_op jit(solution)/shard_map/all_to_all | solution.py:41
  231.5 0.8 dynamic-slice_bitcast_fusion
  232.4 0.2 fusion.37
  232.6 17.2 %all-to-all-done.4 = bf16[16,2,1,2,2048]{4,3,1,2,0:T(2,128)(2,1)S(1)} async-done(((bf16[16,2,1,2,2048]{4,3,1,2,0:T(2,128)(2,1)}), bf16[16,2,1,2,2048]{4,3,1,2,0:T(2,128)(2,1)S(1)}, u32[]{:S(2)}, u32[]{:S(2)}) %all-to-all-start.4) | async-done | bytes 262176 | tf_op jit(solution)/shard_map/all_to_all | solution.py:41
  249.9 0.2 fusion
  250.1 0.1 broadcast_in_dim.39
  250.3 19.5 %all_to_all.33 = bf16[16,16,2048]{2,1,0:T(8,128)(2,1)S(1)} all-to-all(bf16[16,16,2048]{2,1,0:T(8,128)(2,1)S(1)} %broadcast_in_dim.39), channel_id=1, replica_groups=mesh['sp_0'=16,'sp_1'=2,'tp'=16] {'tp'}, dimensions={0} | all-to-all | bytes 2097152 | tf_op jit(solution)/shard_map/all_to_all | solution.py:53
  269.8 1.0 copy.43
  (34 shorter events, 1.0 us)
Async XLA Ops:
  6.5 140.9 %copy-start = (bf16[1,224,2048]{2,1,0:T(8,128)(2,1)S(1)}, bf16[1,224,2048]{2,1,0:T(8,128)(2,1)}, u32[]{:S(2)}) copy-start(bf16[1,224,2048]{2,1,0:T(8,128)(2,1)} %param.19) | copy-start | bytes 2752516
  6.5 6.0 %copy-start.2 = (s32[256,2]{0,1:T(2,128)S(1)}, s32[256,2]{0,1:T(2,128)}, u32[]{:S(2)}) copy-start(s32[256,2]{0,1:T(2,128)} %param.15) | copy-start | bytes 6148
  6.5 9.1 %copy-start.6 = (f32[128]{0:T(128)S(1)}, f32[128]{0:T(128)}, u32[]{:S(2)}) copy-start(f32[128]{0:T(128)} %param.13) | copy-start | bytes 1540
  6.5 9.1 %copy-start.5 = (bf16[512,128]{1,0:T(8,128)(2,1)S(1)}, bf16[512,128]{1,0:T(8,128)(2,1)}, u32[]{:S(2)}) copy-start(bf16[512,128]{1,0:T(8,128)(2,1)} %param.12) | copy-start | bytes 393220
  10.5 5.1 %collective-permute-start = (bf16[16,512]{1,0:T(8,128)(2,1)S(1)}, bf16[16,512]{1,0:T(8,128)(2,1)S(1)}, u32[]{:S(2)}, u32[]{:S(2)}) collective-permute-start(bf16[16,512]{1,0:T(8,128)(2,1)S(1)} %slice.69), channel_id=1, source_target_pairs={{0,16},{16,32},{32,48},{48,64},{64,80},{80,96},{96,112},{112,128},... | collective-permute-start | bytes 49160 | tf_op jit(solution)/shard_map/ppermute | solution.py:17
  15.7 25.8 %copy-start.1 = (f32[2048]{0:T(1024)S(1)}, f32[2048]{0:T(1024)}, u32[]{:S(2)}) copy-start(f32[2048]{0:T(1024)} %param.14) | copy-start | bytes 24580
  26.6 14.7 %all-to-all-start = ((bf16[16,16,128]{2,1,0:T(8,128)(2,1)}), bf16[16,16,128]{2,1,0:T(8,128)(2,1)S(1)}, u32[]{:S(2)}, u32[]{:S(2)}) async-start(bf16[16,16,128]{2,1,0:T(8,128)(2,1)} %constant_dynamic-update-slice_fusion), calls=%async_computation | async-start | bytes 131072 | tf_op jit(solution)/shard_map/all_to_all | solution.py:120
  33.6 102.0 %all-gather.2.cloned.1.call-start = ((), (), s32[]{:S(2)}) async-start(), calls=%async_computation.6 | async-start | bytes 4456448 | tf_op jit(solution)/shard_map/all_gather | solution.py:135
  79.7 63.2 %copy-start.3 = (bf16[1,2048,224]{1,2,0:T(8,128)(2,1)S(1)}, bf16[1,2048,224]{1,2,0:T(8,128)(2,1)}, u32[]{:S(2)}) copy-start(bf16[1,2048,224]{1,2,0:T(8,128)(2,1)} %param.17) | copy-start | bytes 2752516
  142.9 4.6 %copy-start.4 = (bf16[1,2048,224]{1,2,0:T(8,128)(2,1)S(1)}, bf16[1,2048,224]{1,2,0:T(8,128)(2,1)}, u32[]{:S(2)}) copy-start(bf16[1,2048,224]{1,2,0:T(8,128)(2,1)} %param.18) | copy-start | bytes 2752516
  218.8 31.0 %all-to-all-start.4 = ((bf16[16,2,1,2,2048]{4,3,1,2,0:T(2,128)(2,1)}), bf16[16,2,1,2,2048]{4,3,1,2,0:T(2,128)(2,1)S(1)}, u32[]{:S(2)}, u32[]{:S(2)}) async-start(bf16[16,2,1,2,2048]{4,3,1,2,0:T(2,128)(2,1)} %copy.20), calls=%async_computation.4 | async-start | bytes 524288 | tf_op jit(solution)/shard_map/all_to_all | solution.py:41
Sparse Core Ops, SparseCore 0:
  79.8 55.8 all-gather.1
